TPU v7x, 32 devices: a whole 2x2x4 slice. The times are simulated.
32 devices in a mesh: sp: 16 (over z, y, x), tp: 2 (over core).
Axes of the slice: x: 2, y: 2, z: 4, core: 2. Of those that a mesh axis runs over, the one named last changes fastest.
Arguments:
- tokens: bfloat16 [4096, 2048], P('sp'), may hold values from -6 to 6
- query_weight: bfloat16 [2, 2048, 512], P(None, None, 'tp'), may hold values from -0.125 to 0.125
- key_weight: bfloat16 [2, 2048, 512], P(None, None, 'tp'), may hold values from -0.125 to 0.125
- value_weight: bfloat16 [2, 2048, 512], P(None, None, 'tp'), may hold values from -0.125 to 0.125
- out_weight: bfloat16 [2, 512, 2048], replicated, may hold values from -1.5 to 1.5
- rel_table: float32 [2, 8, 257], P(None, 'tp'), may hold values from -5 to 262
- norm_gain: float32 [2, 2048], replicated, may hold values from 0.1 to 1.9
- norm_bias: float32 [2, 2048], replicated, may hold values from -1.5 to 1.5
Outputs:
- encoded: bfloat16 [4096, 2048], P('sp', 'tp')
All inputs are finite; a program needn't handle non-finite values.
Results may differ from a plain program's by a relative error of at most 0.0095.
Values may be sent and summed in bfloat16 or wider, within the bound.
A program may use at most 64 MiB of HBM per device.

v0:
```python
import jax
import jax.numpy as jnp
from jax import lax
from jax.sharding import PartitionSpec as P

SEG = 64
LEFT = 4
CLIP = 128
LAYERS = 2


residual_scale = 2.0**0.5
norm_eps = 1e-05
masked_score = -1e30


def passed_along(value, axis, steps):
    count = lax.axis_size(axis)
    initial, last = (max(0, -steps), min(count, count - steps))
    return lax.ppermute(value, axis, [(source, source + steps) for source in range(initial, last)])


def post_norm(previous, mixed, gain, shift):
    total = residual_scale * previous.astype(jnp.float32) + mixed
    mean = jnp.mean(total, -1, keepdims=True)
    centred = total - mean
    variance = jnp.mean(centred * centred, -1, keepdims=True)
    return (centred * lax.rsqrt(variance + norm_eps) * gain + shift).astype(jnp.bfloat16)


def band_bias(table, reach, band):
    head_count = table.shape[0]
    table_width = table.shape[1]
    span_count = band + SEG - 1
    offsets = jnp.arange(span_count, dtype=jnp.int32)
    distance = reach + SEG - 1 - offsets
    column = jnp.clip(distance, -CLIP, CLIP) + CLIP
    onehot = (column[None, :] == jnp.arange(table_width, dtype=jnp.int32)[:, None]).astype(
        jnp.float32
    )
    by_offset = jnp.dot(table, onehot, precision=lax.Precision.HIGHEST)
    padded = jnp.concatenate([by_offset, jnp.zeros((head_count, 1), jnp.float32)], axis=1)
    period = span_count + 1
    tiled = jnp.tile(padded, (1, SEG))
    skewed = tiled[:, SEG - 1 : SEG - 1 + SEG * (period - 1)].reshape(head_count, SEG, period - 1)
    return skewed[:, :, :band]


def attend(query, keys_ext, values_ext, table, offset):
    tok_rows = query.shape[0]
    head_count = table.shape[0]
    head_size = query.shape[1] // head_count
    seg_count = tok_rows // SEG
    reach = LEFT * SEG
    band = reach + SEG
    query_blocks = query.reshape(seg_count, SEG, head_count, head_size)
    key_blocks = keys_ext.reshape(seg_count + LEFT, SEG, head_count, head_size)
    value_blocks = values_ext.reshape(seg_count + LEFT, SEG, head_count, head_size)
    key_band = jnp.concatenate(
        [key_blocks[step : step + seg_count] for step in range(LEFT + 1)], axis=1
    )
    value_band = jnp.concatenate(
        [value_blocks[step : step + seg_count] for step in range(LEFT + 1)], axis=1
    )
    scores = jnp.einsum(
        "cqhd,ckhd->hcqk", query_blocks, key_band, preferred_element_type=jnp.float32
    )
    scores = scores * head_size ** (-0.5)
    bias = band_bias(table, reach, band)
    scores = scores + bias[:, None]
    key_position = (
        offset
        - reach
        + jnp.arange(seg_count, dtype=jnp.int32)[:, None] * SEG
        + jnp.arange(band, dtype=jnp.int32)[None, :]
    )
    scores = jnp.where((key_position >= 0)[None, :, None, :], scores, masked_score)
    peak = jnp.max(scores, -1, keepdims=True)
    expo = jnp.exp(scores - peak)
    weights = (expo / jnp.sum(expo, -1, keepdims=True)).astype(jnp.bfloat16)
    attended = jnp.einsum(
        "hcqk,ckhd->cqhd", weights, value_band, preferred_element_type=jnp.float32
    )
    return attended.astype(jnp.bfloat16).reshape(tok_rows, head_count * head_size)


def body(
    tokens, query_weight, key_weight, value_weight, out_weight, rel_table, norm_gain, norm_bias
):
    tok_rows = tokens.shape[0]
    model_width = tokens.shape[1]
    offset = lax.axis_index("sp") * tok_rows
    hidden = tokens
    for layer_index in range(LAYERS):
        query = jnp.dot(
            hidden, query_weight[layer_index], preferred_element_type=jnp.float32
        ).astype(jnp.bfloat16)
        keys = jnp.dot(hidden, key_weight[layer_index], preferred_element_type=jnp.float32).astype(
            jnp.bfloat16
        )
        values = jnp.dot(
            hidden, value_weight[layer_index], preferred_element_type=jnp.float32
        ).astype(jnp.bfloat16)
        earlier_keys, earlier_values = passed_along((keys, values), "sp", 1)
        keys_ext = jnp.concatenate([earlier_keys, keys], axis=0)
        values_ext = jnp.concatenate([earlier_values, values], axis=0)
        attended = attend(query, keys_ext, values_ext, rel_table[layer_index], offset)
        project_weight = out_weight[layer_index]
        mixed = jnp.dot(
            lax.all_gather(attended, "tp", axis=1, tiled=True),
            project_weight,
            preferred_element_type=jnp.float32,
        )
        hidden = post_norm(hidden, mixed, norm_gain[layer_index], norm_bias[layer_index])
    width = model_width // lax.axis_size("tp")
    return lax.dynamic_slice_in_dim(hidden, lax.axis_index("tp") * width, width, 1)


def solution(mesh):
    return jax.shard_map(
        body,
        mesh=mesh,
        in_specs=(
            P("sp", None),
            P(None, None, "tp"),
            P(None, None, "tp"),
            P(None, None, "tp"),
            P(),
            P(None, "tp", None),
            P(),
            P(),
        ),
        out_specs=P("sp", "tp"),
        check_vma=False,
    )
```

profile of v0, /device:TPU:25, one launch (start us, length us, event | category | flops | bytes accessed | tf_op | source)
XLA Modules:
  0.0 68.5 jit_solution(3584044833561572752)
XLA Ops:
  0.0 2.1 %convolution_convert_fusion.5 = bf16[256,256]{1,0:T(8,128)(2,1)S(1)} fusion(bf16[256,2048]{1,0:T(8,128)(2,1)} %param.8, bf16[2,2048,256]{2,1,0:T(8,128)(2,1)} %param.10), kind=kOutput, calls=%fused_computation.26 | convolution fusion | flops 268500992 | bytes 2228224 | tf_op jit(solution)/shard_map/dot_general | solution.py:98
  2.1 3.1 %collective-permute-start.1 = (bf16[256,256]{1,0:T(8,128)(2,1)S(1)}, bf16[256,256]{1,0:T(8,128)(2,1)S(1)}, u32[]{:S(2)}, u32[]{:S(2)}) collective-permute-start(bf16[256,256]{1,0:T(8,128)(2,1)S(1)} %convolution_convert_fusion.5), channel_id=1, source_target_pairs={{0,2},{2,4},{4,6},{6,8},{8,10},{10,12},{12,14},{14,16},{16,18},{18... | collective-permute-start | bytes 393224 | tf_op jit(solution)/shard_map/ppermute | solution.py:20
  5.3 1.7 %convolution_convert_fusion.7 = bf16[256,256]{1,0:T(8,128)(2,1)S(1)} fusion(bf16[256,2048]{1,0:T(8,128)(2,1)} %param.8, bf16[2,2048,256]{2,1,0:T(8,128)(2,1)S(1)} %copy-done.6), kind=kOutput, calls=%fused_computation.28 | convolution fusion | flops 268500992 | bytes 2228224 | tf_op jit(solution)/shard_map/dot_general | solution.py:101
  7.0 3.1 %collective-permute-start = (bf16[256,256]{1,0:T(8,128)(2,1)S(1)}, bf16[256,256]{1,0:T(8,128)(2,1)S(1)}, u32[]{:S(2)}, u32[]{:S(2)}) collective-permute-start(bf16[256,256]{1,0:T(8,128)(2,1)S(1)} %convolution_convert_fusion.7), channel_id=1, source_target_pairs={{0,2},{2,4},{4,6},{6,8},{8,10},{10,12},{12,14},{14,16},{16,18},{18... | collective-permute-start | bytes 393224 | tf_op jit(solution)/shard_map/ppermute | solution.py:20
  10.7 2.0 %convolution_convert_fusion.6 = bf16[256,256]{1,0:T(8,128)(2,1)S(1)} fusion(bf16[256,2048]{1,0:T(8,128)(2,1)} %param.8, bf16[2,2048,256]{2,1,0:T(8,128)(2,1)} %param.9), kind=kOutput, calls=%fused_computation.27 | convolution fusion | flops 268500992 | bytes 2228224 | tf_op jit(solution)/shard_map/dot_general | solution.py:95
  13.9 1.2 %reshape.113 = f32[4,64,383]{2,1,0:T(8,128)} reshape(f32[4,24512]{1,0:T(4,128)S(1)} %slice.216) | data formatting | bytes 784384 | tf_op jit(solution)/shard_map/reshape | solution.py:45
  15.2 0.9 %reshape.112 = bf16[4,64,4,64]{3,2,1,0:T(4,128)(2,1)} reshape(bf16[256,256]{1,0:T(8,128)(2,1)S(1)} %convolution_convert_fusion.6) | data formatting | bytes 262144 | tf_op jit(solution)/shard_map/reshape | solution.py:56
  16.8 1.2 %reshape.116 = f32[4,64,383]{2,1,0:T(8,128)} reshape(f32[4,24512]{1,0:T(4,128)S(1)} %slice.226) | data formatting | bytes 784384 | tf_op jit(solution)/shard_map/reshape | solution.py:45
  21.1 0.6 concatenate.33
  21.7 2.9 %fusion.61 = (f32[4,4,64]{2,1,0:T(4,128)S(1)}, f32[4,4,64,320]{3,2,1,0:T(8,128)}) fusion(bf16[4,320,4,64]{1,3,0,2:T(8,128)(2,1)S(1)} %concatenate.33, f32[4,64,320]{2,1,0:T(8,128)} %bitcast.69, pred[4,320]{1,0:T(4,128)(4,1)S(1)} %add_compare_fusion, bf16[4,64,4,64]{3,2,1,0:T(4,128)(2,1)} %reshape.112), kind=kOutput, calls=%fused_computation.104 | convolution fusion | flops 43581760 | bytes 2430208 | tf_op jit(solution)/shard_map/sub | solution.py:79
  25.2 2.0 %fusion.10 = bf16[4,64,4,64]{1,3,2,0:T(8,128)(2,1)S(1)} fusion(bf16[4,320,4,64]{1,3,2,0:T(8,128)(2,1)S(1)} %concatenate.31, f32[4,4,64,320]{3,2,1,0:T(8,128)} %get-tuple-element.24, f32[4,4,64]{2,1,0:T(4,128)S(1)} %get-tuple-element.23), kind=kOutput, calls=%fused_computation.21 | convolution fusion | flops 42663936 | bytes 2101248 | tf_op jit(solution)/shard_map/hcqk,ckhd->cqhd/dot_general | solution.py:81
  27.6 2.9 %all_gather.6 = bf16[256,512]{1,0:T(8,128)(2,1)S(1)} all-gather(bf16[256,256]{1,0:T(8,128)(2,1)S(1)} %reshape.114), channel_id=1, replica_groups=mesh['sp'=16,'tp'=2] {'tp'}, dimensions={1}, use_global_device_ids=true | all-gather | bytes 393216 | tf_op jit(solution)/shard_map/all_gather | solution.py:110
  30.4 2.5 %fusion.64 = (f32[256]{0:T(256)S(1)}, f32[256,2048]{1,0:T(8,128)S(1)}) fusion(bf16[256,512]{1,0:T(8,128)(2,1)S(1)} %all_gather.6, bf16[2,512,2048]{2,1,0:T(8,128)(2,1)} %param.12, bf16[256,2048]{1,0:T(8,128)(2,1)S(1)} %copy-done.9), kind=kOutput, calls=%fused_computation.105 | convolution fusion | flops 538967808 | bytes 5506048 | tf_op jit(solution)/shard_map/dot_general | solution.py:109
  33.8 1.1 %copy-done.5 = bf16[2,2048,256]{2,1,0:T(8,128)(2,1)S(1)} copy-done((bf16[2,2048,256]{2,1,0:T(8,128)(2,1)S(1)}, bf16[2,2048,256]{2,1,0:T(8,128)(2,1)}, u32[]{:S(2)}) %copy-start.5) | copy-done | bytes 2097176
  35.3 1.1 %copy-done.7 = bf16[2,2048,256]{2,1,0:T(8,128)(2,1)S(1)} copy-done((bf16[2,2048,256]{2,1,0:T(8,128)(2,1)S(1)}, bf16[2,2048,256]{2,1,0:T(8,128)(2,1)}, u32[]{:S(2)}) %copy-start.7) | copy-done | bytes 2097176
  36.9 3.1 %collective-permute-start.3 = (bf16[256,256]{1,0:T(8,128)(2,1)S(1)}, bf16[256,256]{1,0:T(8,128)(2,1)S(1)}, u32[]{:S(2)}, u32[]{:S(2)}) collective-permute-start(bf16[256,256]{1,0:T(8,128)(2,1)S(1)} %convolution_convert_fusion.2), channel_id=1, source_target_pairs={{0,2},{2,4},{4,6},{6,8},{8,10},{10,12},{12,14},{14,16},{16,18},{18... | collective-permute-start | bytes 393224 | tf_op jit(solution)/shard_map/ppermute | solution.py:20
  40.0 2.1 %collective-permute-start.2 = (bf16[256,256]{1,0:T(8,128)(2,1)S(1)}, bf16[256,256]{1,0:T(8,128)(2,1)S(1)}, u32[]{:S(2)}, u32[]{:S(2)}) collective-permute-start(bf16[256,256]{1,0:T(8,128)(2,1)S(1)} %convolution_convert_fusion.4), channel_id=1, source_target_pairs={{0,2},{2,4},{4,6},{6,8},{8,10},{10,12},{12,14},{14,16},{16,18},{18... | collective-permute-start | bytes 393224 | tf_op jit(solution)/shard_map/ppermute | solution.py:20
  43.2 0.9 %reshape.115 = bf16[4,64,4,64]{3,2,1,0:T(4,128)(2,1)} reshape(bf16[256,256]{1,0:T(8,128)(2,1)S(1)} %convolution_convert_fusion.3) | data formatting | bytes 262144 | tf_op jit(solution)/shard_map/reshape | solution.py:56
  44.2 1.0 %collective-permute-done.3 = bf16[256,256]{1,0:T(8,128)(2,1)S(1)} collective-permute-done((bf16[256,256]{1,0:T(8,128)(2,1)S(1)}, bf16[256,256]{1,0:T(8,128)(2,1)S(1)}, u32[]{:S(2)}, u32[]{:S(2)}) %collective-permute-start.3) | collective-permute-done | bytes 131104 | tf_op jit(solution)/shard_map/ppermute | solution.py:20
  46.9 1.2 %collective-permute-done.2 = bf16[256,256]{1,0:T(8,128)(2,1)S(1)} collective-permute-done((bf16[256,256]{1,0:T(8,128)(2,1)S(1)}, bf16[256,256]{1,0:T(8,128)(2,1)S(1)}, u32[]{:S(2)}, u32[]{:S(2)}) %collective-permute-start.2) | collective-permute-done | bytes 131104 | tf_op jit(solution)/shard_map/ppermute | solution.py:20
  48.1 0.7 %pad_maximum_fusion.1 = (bf16[256,256]{1,0:T(8,128)(2,1)}, bf16[256,256]{1,0:T(8,128)(2,1)S(1)}, bf16[256,256]{1,0:T(8,128)(2,1)}) fusion(bf16[256,256]{1,0:T(8,128)(2,1)S(1)} %convolution_convert_fusion.4, bf16[256,256]{1,0:T(8,128)(2,1)S(1)} %collective-permute-done.2), kind=kLoop, calls=%fused_computation.82 | loop fusion | flops 786432 | bytes 655360 | tf_op jit(solution)/shard_map/concatenate | solution.py:106
  49.2 1.1 %slice.188 = bf16[4,64,4,64]{3,2,1,0:T(4,128)(2,1)S(1)} reshape(bf16[256,256]{1,0:T(8,128)(2,1)} %get-tuple-element.12) | data formatting | bytes 262144 | tf_op jit(solution)/shard_map/slice | solution.py:63
  50.5 1.1 %slice.190 = bf16[4,64,4,64]{3,2,1,0:T(4,128)(2,1)S(1)} reshape(bf16[256,256]{1,0:T(8,128)(2,1)} %get-tuple-element.10) | data formatting | bytes 262144 | tf_op jit(solution)/shard_map/slice | solution.py:63
  51.6 0.9 %copy.49 = bf16[4,64,4,64]{1,3,2,0:T(8,128)(2,1)} copy(bf16[4,64,4,64]{3,2,1,0:T(4,128)(2,1)S(1)} %slice.190) | data formatting | bytes 262144 | tf_op jit(solution)/shard_map/slice | solution.py:63
  52.6 0.9 %copy.46 = bf16[4,64,4,64]{1,3,2,0:T(8,128)(2,1)} copy(bf16[4,64,4,64]{3,2,1,0:T(4,128)(2,1)S(1)} %slice.184) | data formatting | bytes 262144 | tf_op jit(solution)/shard_map/slice | solution.py:63
  53.5 1.3 %concatenate.38 = bf16[4,320,4,64]{1,3,0,2:T(8,128)(2,1)} concatenate(bf16[4,64,4,64]{1,3,0,2:T(8,128)(2,1)S(1)} %copy.51, bf16[4,64,4,64]{1,3,0,2:T(8,128)(2,1)S(1)} %copy.52, bf16[4,64,4,64]{1,3,0,2:T(8,128)(2,1)S(1)} %copy.53, bf16[4,64,4,64]{1,3,0,2:T(8,128)(2,1)S(1)} %copy.54, bf16[4,64,4,64]{1,3,0,2:T(8,128)(2,1)S(1)} %copy.55), dimensions={1} | concatenate | bytes 1310720 | tf_op jit(solution)/shard_map/concatenate | solution.py:59
  54.8 3.7 %fusion.65 = (f32[4,4,64]{2,1,0:T(4,128)}, f32[4,4,64,320]{3,2,1,0:T(8,128)}) fusion(bf16[4,320,4,64]{1,3,0,2:T(8,128)(2,1)} %concatenate.38, f32[4,64,320]{2,1,0:T(8,128)S(1)} %bitcast.68, pred[4,320]{1,0:T(4,128)(4,1)S(1)} %add_compare_fusion, bf16[4,64,4,64]{3,2,1,0:T(4,128)(2,1)} %reshape.115), kind=kOutput, calls=%fused_computation.106 | convolution fusion | flops 43581760 | bytes 2430208 | tf_op jit(solution)/shard_map/sub | solution.py:79
  58.5 0.6 concatenate.36
  59.2 1.9 %fusion.11 = bf16[4,64,4,64]{1,3,2,0:T(8,128)(2,1)S(1)} fusion(bf16[4,320,4,64]{1,3,2,0:T(8,128)(2,1)S(1)} %concatenate.36, f32[4,4,64,320]{3,2,1,0:T(8,128)} %get-tuple-element.28, f32[4,4,64]{2,1,0:T(4,128)S(1)} %copy-done.11), kind=kOutput, calls=%fused_computation.22 | convolution fusion | flops 42663936 | bytes 2101248 | tf_op jit(solution)/shard_map/hcqk,ckhd->cqhd/dot_general | solution.py:81
  61.5 3.1 %all_gather.7 = bf16[256,512]{1,0:T(8,128)(2,1)S(1)} all-gather(bf16[256,256]{1,0:T(8,128)(2,1)S(1)} %reshape.117), channel_id=1, replica_groups=mesh['sp'=16,'tp'=2] {'tp'}, dimensions={1}, use_global_device_ids=true | all-gather | bytes 393216 | tf_op jit(solution)/shard_map/all_gather | solution.py:110
  64.7 2.4 %fusion.68 = (f32[256]{0:T(256)S(1)}, f32[256,2048]{1,0:T(8,128)S(1)}) fusion(bf16[256,512]{1,0:T(8,128)(2,1)S(1)} %all_gather.7, bf16[2,512,2048]{2,1,0:T(8,128)(2,1)} %param.12, bf16[256,2048]{1,0:T(8,128)(2,1)S(1)} %add_convert_fusion), kind=kOutput, calls=%fused_computation.107 | convolution fusion | flops 538967808 | bytes 5506048 | tf_op jit(solution)/shard_map/dot_general | solution.py:109
  67.5 1.0 %fusion.14 = bf16[256,1024]{1,0:T(8,128)(2,1)} fusion(f32[256,2048]{1,0:T(8,128)S(1)} %get-tuple-element.6, s32[]{:T(128)S(6)} %select_n.12, f32[1024]{0:T(1024)S(1)} %dynamic-slice.1, f32[1024]{0:T(1024)S(1)} %dynamic-slice, f32[256]{0:T(256)S(1)} %add_rsqrt_fusion), kind=kLoop, calls=%fused_computation.34 | loop fusion | flops 1048576 | bytes 1582084 | tf_op jit(solution)/shard_map/convert_element_type | solution.py:28
  (95 shorter events, 12.5 us)
Async XLA Ops:
  0.0 5.3 %copy-start.6 = (bf16[2,2048,256]{2,1,0:T(8,128)(2,1)S(1)}, bf16[2,2048,256]{2,1,0:T(8,128)(2,1)}, u32[]{:S(2)}) copy-start(bf16[2,2048,256]{2,1,0:T(8,128)(2,1)} %param.11) | copy-start | bytes 6291460
  0.0 10.1 %copy-start.10 = (f32[2,4,257]{2,1,0:T(4,128)S(1)}, f32[2,4,257]{2,1,0:T(4,128)}, u32[]{:S(2)}) copy-start(f32[2,4,257]{2,1,0:T(4,128)} %param.13) | copy-start | bytes 24676
  2.1 15.8 %collective-permute-start.1 = (bf16[256,256]{1,0:T(8,128)(2,1)S(1)}, bf16[256,256]{1,0:T(8,128)(2,1)S(1)}, u32[]{:S(2)}, u32[]{:S(2)}) collective-permute-start(bf16[256,256]{1,0:T(8,128)(2,1)S(1)} %convolution_convert_fusion.5), channel_id=1, source_target_pairs={{0,2},{2,4},{4,6},{6,8},{8,10},{10,12},{12,14},{14,16},{16,18},{18... | collective-permute-start | bytes 393224 | tf_op jit(solution)/shard_map/ppermute | solution.py:20
  6.9 5.7 %copy-start.3 = (f32[2,2048]{1,0:T(2,128)S(1)}, f32[2,2048]{1,0:T(2,128)}, u32[]{:S(2)}) copy-start(f32[2,2048]{1,0:T(2,128)} %param.14) | copy-start | bytes 49156
  7.0 5.7 %copy-start.4 = (f32[2,2048]{1,0:T(2,128)S(1)}, f32[2,2048]{1,0:T(2,128)}, u32[]{:S(2)}) copy-start(f32[2,2048]{1,0:T(2,128)} %param.15) | copy-start | bytes 49156
  7.0 12.6 %collective-permute-start = (bf16[256,256]{1,0:T(8,128)(2,1)S(1)}, bf16[256,256]{1,0:T(8,128)(2,1)S(1)}, u32[]{:S(2)}, u32[]{:S(2)}) collective-permute-start(bf16[256,256]{1,0:T(8,128)(2,1)S(1)} %convolution_convert_fusion.7), channel_id=1, source_target_pairs={{0,2},{2,4},{4,6},{6,8},{8,10},{10,12},{12,14},{14,16},{16,18},{18... | collective-permute-start | bytes 393224 | tf_op jit(solution)/shard_map/ppermute | solution.py:20
  25.2 5.3 %copy-start.9 = (bf16[256,2048]{1,0:T(8,128)(2,1)S(1)}, bf16[256,2048]{1,0:T(8,128)(2,1)}, u32[]{:S(2)}) copy-start(bf16[256,2048]{1,0:T(8,128)(2,1)} %param.8) | copy-start | bytes 3145732
  33.3 1.6 %copy-start.5 = (bf16[2,2048,256]{2,1,0:T(8,128)(2,1)S(1)}, bf16[2,2048,256]{2,1,0:T(8,128)(2,1)}, u32[]{:S(2)}) copy-start(bf16[2,2048,256]{2,1,0:T(8,128)(2,1)} %param.10) | copy-start | bytes 6291460
  34.9 1.6 %copy-start.7 = (bf16[2,2048,256]{2,1,0:T(8,128)(2,1)S(1)}, bf16[2,2048,256]{2,1,0:T(8,128)(2,1)}, u32[]{:S(2)}) copy-start(bf16[2,2048,256]{2,1,0:T(8,128)(2,1)} %param.11) | copy-start | bytes 6291460
  34.9 7.3 %copy-start.8 = (bf16[2,2048,256]{2,1,0:T(8,128)(2,1)S(1)}, bf16[2,2048,256]{2,1,0:T(8,128)(2,1)}, u32[]{:S(2)}) copy-start(bf16[2,2048,256]{2,1,0:T(8,128)(2,1)} %param.9) | copy-start | bytes 6291460
  36.9 8.4 %collective-permute-start.3 = (bf16[256,256]{1,0:T(8,128)(2,1)S(1)}, bf16[256,256]{1,0:T(8,128)(2,1)S(1)}, u32[]{:S(2)}, u32[]{:S(2)}) collective-permute-start(bf16[256,256]{1,0:T(8,128)(2,1)S(1)} %convolution_convert_fusion.2), channel_id=1, source_target_pairs={{0,2},{2,4},{4,6},{6,8},{8,10},{10,12},{12,14},{14,16},{16,18},{18... | collective-permute-start | bytes 393224 | tf_op jit(solution)/shard_map/ppermute | solution.py:20
  40.0 8.1 %collective-permute-start.2 = (bf16[256,256]{1,0:T(8,128)(2,1)S(1)}, bf16[256,256]{1,0:T(8,128)(2,1)S(1)}, u32[]{:S(2)}, u32[]{:S(2)}) collective-permute-start(bf16[256,256]{1,0:T(8,128)(2,1)S(1)} %convolution_convert_fusion.4), channel_id=1, source_target_pairs={{0,2},{2,4},{4,6},{6,8},{8,10},{10,12},{12,14},{14,16},{16,18},{18... | collective-permute-start | bytes 393224 | tf_op jit(solution)/shard_map/ppermute | solution.py:20
  53.5 1.3 %copy-start.2 = (f32[4,64,383]{2,1,0:T(8,128)S(1)}, f32[4,64,383]{2,1,0:T(8,128)}, u32[]{:S(2)}) copy-start(f32[4,64,383]{2,1,0:T(8,128)} %reshape.116) | copy-start | bytes 1176580
  54.8 3.7 %copy-start = (bf16[4,64,4,64]{1,3,2,0:T(8,128)(2,1)S(1)}, bf16[4,64,4,64]{1,3,2,0:T(8,128)(2,1)}, u32[]{:S(2)}) copy-start(bf16[4,64,4,64]{1,3,2,0:T(8,128)(2,1)} %copy.49) | copy-start | bytes 393220
  54.8 3.7 %copy-start.1 = (bf16[4,64,4,64]{1,3,2,0:T(8,128)(2,1)S(1)}, bf16[4,64,4,64]{1,3,2,0:T(8,128)(2,1)}, u32[]{:S(2)}) copy-start(bf16[4,64,4,64]{1,3,2,0:T(8,128)(2,1)} %copy.46) | copy-start | bytes 393220
  58.5 0.7 %copy-start.11 = (f32[4,4,64]{2,1,0:T(4,128)S(1)}, f32[4,4,64]{2,1,0:T(4,128)}, u32[]{:S(2)}) copy-start(f32[4,4,64]{2,1,0:T(4,128)} %get-tuple-element.27) | copy-start | bytes 12292
where the time goes:
time: 69 us; the launch traced here: 68.5 us
  matrix products  22.8 us (33%)
  local copies, waits for them, and re-layouts  22.1 us (32%)
  starting transfers between devices  11.5 us (17%)
  blocking collectives  6.01 us (9%)
  other arithmetic  3.1 us (4%)
  waiting for transfers between devices  2.26 us (3%)
    ppermute x4, starting transfers between devices, passed_along(): lax.ppermute(value, axis, [(source, source + steps) for source in range(i...  11.5 us
    slice x20, local copies, waits for them, and re-layouts, attend(): value_blocks[step:step + seg_count]  6.76 us
    sub x2, matrix products, attend(): expo = jnp.exp(scores - peak)  6.55 us
    all_gather x2, blocking collectives, body(): lax.all_gather(attended, 'tp', axis=1, tiled=True)  6.01 us
    dot_general x2, matrix products, body(): jnp.dot(lax.all_gather(attended, 'tp', axis=1, tiled=True), project_weigh...  4.86 us
    dot_general x2, matrix products, attend(): jnp.einsum('hcqk,ckhd->cqhd', weights, value_band, preferred_element_type...  3.88 us
    slice x20, local copies, waits for them, and re-layouts, attend(): key_blocks[step:step + seg_count]  3.85 us
    unnamed x28, local copies, waits for them, and re-layouts  2.99 us
  transfers between devices with their start and end apart: 4, of which 2 were waited for; matrix products, arithmetic and copies ran while one was open for 21% of the time, Pallas kernels for 0%

commit v1 on v0

v1 whole, which is shorter than its diff:
```python
import functools

import jax
import jax.numpy as jnp
from jax import lax
from jax.experimental import pallas as pl
from jax.experimental.pallas import tpu as pltpu
from jax.sharding import PartitionSpec as P

SEG = 64
LEFT = 4
CLIP = 128
LAYERS = 2
CHUNKS = 2
LANES = 128

residual_scale = 2.0**0.5
norm_eps = 1e-05
masked_score = -1e30
MESH = pl.DeviceIdType.MESH


def kernel(
    sp_count,
    heads,
    tokens,
    wq_hbm,
    wk_hbm,
    wv_hbm,
    wo_hbm,
    table,
    gain,
    shift,
    out,
    x0,
    x1,
    wq,
    wk,
    wv,
    wo,
    query,
    kx,
    vx,
    att,
    total,
    bias,
    padded,
    x_sem,
    w_sem,
    halo_send,
    halo_recv,
    pair_send,
    pair_recv,
):
    rows, model = x0.shape
    width = query.shape[1]
    head_size = width // heads
    reach = LEFT * SEG
    band = reach + SEG
    chunk = rows // CHUNKS
    sp = lax.axis_index("sp")
    tp = lax.axis_index("tp")
    has_next = sp < sp_count - 1
    has_prev = sp > 0
    order = list(range(CHUNKS))[::-1]

    def x_copy(c):
        part = pl.ds(c * chunk, chunk)
        return pltpu.make_async_copy(tokens.at[part], x0.at[part], x_sem.at[c])

    def w_copy(kind, layer):
        source = (wk_hbm, wv_hbm, wq_hbm, wo_hbm)[kind]
        target = (wk, wv, wq, wo)[kind]
        return pltpu.make_async_copy(
            source.at[layer], target.at[layer], w_sem.at[kind, layer]
        )

    def halo_copy(kind, layer, c):
        buffer = (kx, vx)[kind]
        return pltpu.make_async_remote_copy(
            src_ref=buffer.at[layer, pl.ds(reach + c * chunk, chunk)],
            dst_ref=buffer.at[layer, pl.ds(c * chunk, chunk)],
            send_sem=halo_send.at[kind, layer, c],
            recv_sem=halo_recv.at[kind, layer, c],
            device_id=(jnp.minimum(sp + 1, sp_count - 1), tp),
            device_id_type=MESH,
        )

    def pair_copy(layer, c):
        block = att.at[layer, tp, pl.ds(c * chunk, chunk)]
        return pltpu.make_async_remote_copy(
            src_ref=block,
            dst_ref=block,
            send_sem=pair_send.at[layer, c],
            recv_sem=pair_recv.at[layer, c],
            device_id=(sp, 1 - tp),
            device_id_type=MESH,
        )

    for c in order:
        x_copy(c).start()
    for kind in range(4):
        w_copy(kind, 0).start()

    barrier = pltpu.get_barrier_semaphore()
    pl.semaphore_signal(barrier, inc=1, device_id=(sp, 1 - tp), device_id_type=MESH)

    @pl.when(has_next)
    def _():
        pl.semaphore_signal(barrier, inc=1, device_id=(sp + 1, tp), device_id_type=MESH)

    @pl.when(has_prev)
    def _():
        pl.semaphore_signal(barrier, inc=1, device_id=(sp - 1, tp), device_id_type=MESH)

    @pl.when(jnp.logical_not(has_prev))
    def _():
        for layer in range(LAYERS):
            kx[layer, :reach, :] = jnp.zeros((reach, width), jnp.bfloat16)
            vx[layer, :reach, :] = jnp.zeros((reach, width), jnp.bfloat16)

    wide = bias.shape[2]
    size = padded.shape[1]
    padded[...] = jnp.zeros_like(padded)
    for layer in range(LAYERS):
        padded[layer * heads : (layer + 1) * heads, : table.shape[2]] = table[layer]
    place = lax.broadcasted_iota(jnp.int32, (size, wide), 1)
    source = lax.broadcasted_iota(jnp.int32, (size, wide), 0)
    onehot = (jnp.clip(band - 1 - place, -CLIP, CLIP) + CLIP == source).astype(jnp.float32)
    by_offset = jnp.dot(
        padded[...], onehot, precision=lax.Precision.HIGHEST, preferred_element_type=jnp.float32
    )
    for layer in range(LAYERS):
        for h in range(heads):
            line = by_offset[layer * heads + h : layer * heads + h + 1, :]
            skewed = pltpu.roll(
                jnp.broadcast_to(line, (SEG, wide)), wide - SEG + 1, 1, stride=1, stride_axis=0
            )
            bias[layer, h * SEG : (h + 1) * SEG, :] = skewed

    pl.semaphore_wait(
        barrier, 1 + has_next.astype(jnp.int32) + has_prev.astype(jnp.int32)
    )

    lane = lax.broadcasted_iota(jnp.int32, (1, width), 1)
    in_head = [
        (lane >= h * head_size) & (lane < (h + 1) * head_size) for h in range(heads)
    ]

    def project(hidden, layer, c, kind):
        part = slice(c * chunk, (c + 1) * chunk)
        weight = (wk, wv, wq)[kind]
        return jnp.dot(
            hidden[part, :], weight[layer], preferred_element_type=jnp.float32
        ).astype(jnp.bfloat16)

    def keys_values(hidden, layer, c):
        for kind in range(2):
            if c == order[0]:
                w_copy(kind, layer).wait()
            buffer = (kx, vx)[kind]
            buffer[layer, reach + c * chunk : reach + (c + 1) * chunk, :] = project(
                hidden, layer, c, kind
            )

            @pl.when(has_next)
            def _():
                halo_copy(kind, layer, c).start()

    def queries(hidden, layer, c):
        if c == order[0]:
            w_copy(2, layer).wait()
        part = slice(c * chunk, (c + 1) * chunk)
        query[part, :] = project(hidden, layer, c, 2) * jnp.bfloat16(head_size**-0.5)

    def attend(layer, c):
        @pl.when(has_prev)
        def _():
            halo_copy(0, layer, c).wait_recv()
            halo_copy(1, layer, c).wait_recv()

        column = lax.broadcasted_iota(jnp.int32, (1, band), 1)
        for seg in range(c * chunk // SEG, (c + 1) * chunk // SEG):
            block = query[seg * SEG : (seg + 1) * SEG, :]
            stacked = jnp.concatenate(
                [jnp.where(in_head[h], block, jnp.zeros_like(block)) for h in range(heads)],
                axis=0,
            )
            keys = kx[layer, seg * SEG : seg * SEG + band, :]
            values = vx[layer, seg * SEG : seg * SEG + band, :]
            scores = lax.dot_general(
                stacked, keys, (((1,), (1,)), ((), ())), preferred_element_type=jnp.float32
            )
            outside = (column < reach - seg * SEG) & jnp.logical_not(has_prev)
            scores = scores + bias[layer, :, :band]
            scores = jnp.where(outside, masked_score, scores)
            peak = jnp.max(scores, -1, keepdims=True)
            expo = jnp.exp(scores - peak)
            norm = jnp.sum(expo, -1, keepdims=True)
            mixed = jnp.dot(
                expo.astype(jnp.bfloat16), values, preferred_element_type=jnp.float32
            )
            mixed = mixed / norm
            own = jnp.zeros((SEG, width), jnp.float32)
            for h in range(heads):
                own = jnp.where(in_head[h], mixed[h * SEG : (h + 1) * SEG, :], own)
            att[layer, tp, seg * SEG : (seg + 1) * SEG, :] = own.astype(jnp.bfloat16)
        pair_copy(layer, c).start()

    def finish(hidden, layer, c):
        pair_copy(layer, c).wait_recv()
        if c == order[0]:
            w_copy(3, layer).wait()
        part = slice(c * chunk, (c + 1) * chunk)
        both = jnp.concatenate([att[layer, 0, part, :], att[layer, 1, part, :]], axis=1)
        total[...] = residual_scale * hidden[part, :].astype(jnp.float32) + jnp.dot(
            both, wo[layer], preferred_element_type=jnp.float32
        )
        step = 16
        for r in range(0, chunk, step):
            value = total[r : r + step, :]
            mean = jnp.sum(value, -1, keepdims=True) * (1.0 / model)
            centred = value - mean
            variance = jnp.sum(centred * centred, -1, keepdims=True) * (1.0 / model)
            scale = lax.rsqrt(variance + norm_eps)
            here = slice(c * chunk + r, c * chunk + r + step)
            if layer < LAYERS - 1:
                x1[here, :] = (
                    centred * scale * gain[layer : layer + 1, :] + shift[layer : layer + 1, :]
                ).astype(jnp.bfloat16)
            else:
                half = model // 2
                cols = pl.ds(pl.multiple_of(tp * half, half), half)
                out[here, :] = (
                    (total[r : r + step, cols] - mean) * scale * gain[layer : layer + 1, cols]
                    + shift[layer : layer + 1, cols]
                ).astype(jnp.bfloat16)

    for c in order:
        x_copy(c).wait()
        keys_values(x0, 0, c)
    for kind in range(4):
        w_copy(kind, 1).start()
    for c in order:
        queries(x0, 0, c)
    for c in order:
        attend(0, c)
        finish(x0, 0, c)
        keys_values(x1, 1, c)
        queries(x1, 1, c)
    for c in order:
        attend(1, c)
        finish(x1, 1, c)

    for layer in range(LAYERS):
        for c in order:
            pair_copy(layer, c).wait_send()

    @pl.when(has_next)
    def _():
        for layer in range(LAYERS):
            for c in order:
                for kind in range(2):
                    halo_copy(kind, layer, c).wait_send()


def body(
    sp_count, tokens, query_weight, key_weight, value_weight, out_weight, rel_table, norm_gain,
    norm_bias,
):
    rows, model = tokens.shape
    width = query_weight.shape[2]
    heads = rel_table.shape[1]
    reach = LEFT * SEG
    wide = -(-(reach + 2 * SEG - 1) // LANES) * LANES
    size = -(-rel_table.shape[2] // LANES) * LANES
    anywhere = pl.BlockSpec(memory_space=pl.ANY)
    vmem = pl.BlockSpec(memory_space=pltpu.VMEM)
    bf16 = jnp.bfloat16
    return pl.pallas_call(
        functools.partial(kernel, sp_count, heads),
        out_shape=jax.ShapeDtypeStruct((rows, model // 2), bf16),
        in_specs=[anywhere] * 5 + [vmem] * 3,
        out_specs=vmem,
        scratch_shapes=[
            pltpu.VMEM((rows, model), bf16),
            pltpu.VMEM((rows, model), bf16),
            pltpu.VMEM(query_weight.shape, bf16),
            pltpu.VMEM(key_weight.shape, bf16),
            pltpu.VMEM(value_weight.shape, bf16),
            pltpu.VMEM(out_weight.shape, bf16),
            pltpu.VMEM((rows, width), bf16),
            pltpu.VMEM((LAYERS, reach + rows, width), bf16),
            pltpu.VMEM((LAYERS, reach + rows, width), bf16),
            pltpu.VMEM((LAYERS, 2, rows, width), bf16),
            pltpu.VMEM((rows // CHUNKS, model), jnp.float32),
            pltpu.VMEM((LAYERS, heads * SEG, wide), jnp.float32),
            pltpu.VMEM((-(-LAYERS * heads // 8) * 8, size), jnp.float32),
            pltpu.SemaphoreType.DMA((CHUNKS,)),
            pltpu.SemaphoreType.DMA((4, LAYERS)),
            pltpu.SemaphoreType.DMA((2, LAYERS, CHUNKS)),
            pltpu.SemaphoreType.DMA((2, LAYERS, CHUNKS)),
            pltpu.SemaphoreType.DMA((LAYERS, CHUNKS)),
            pltpu.SemaphoreType.DMA((LAYERS, CHUNKS)),
        ],
        compiler_params=pltpu.CompilerParams(
            collective_id=0, has_side_effects=True, vmem_limit_bytes=48 * 1024 * 1024
        ),
    )(
        tokens, query_weight, key_weight, value_weight, out_weight, rel_table, norm_gain, norm_bias
    )


def solution(mesh):
    return jax.shard_map(
        functools.partial(body, mesh.shape["sp"]),
        mesh=mesh,
        in_specs=(
            P("sp", None),
            P(None, None, "tp"),
            P(None, None, "tp"),
            P(None, None, "tp"),
            P(),
            P(None, "tp", None),
            P(),
            P(),
        ),
        out_specs=P("sp", "tp"),
        check_vma=False,
    )
```

time: 69 us -> 30.2 us (0.44)
  matrix products: 22.8 us -> 0 us
  Pallas kernels: 0 us -> 22.4 us
  local copies, waits for them, and re-layouts: 22.1 us -> 7.34 us
  starting transfers between devices: 11.5 us -> 0 us
  blocking collectives: 6.01 us -> 0 us
  other arithmetic: 3.1 us -> 0 us
  waiting for transfers between devices: 2.26 us -> 0 us
    pallas_call x0 -> x1, Pallas kernels: none -> 22.4 us  [body(): pl.pallas_call(functools.partial(kernel, sp_count, heads), out_shape=jax....]
    dot_general x12 -> x0, matrix products: 16.3 us -> none  [the longest x2 4.86 us: body(): jnp.dot(lax.all_gather(attended, 'tp', axis=1, tiled=True), project_weigh...]
    ppermute x4 -> x0, starting transfers between devices: 11.5 us -> none  [passed_along(): lax.ppermute(value, axis, [(source, source + steps) for source in range(i...]
    slice x44 -> x0, local copies, waits for them, and re-layouts: 11.2 us -> none  [the longest x20 6.76 us: attend(): value_blocks[step:step + seg_count]]
    sub x2 -> x0, matrix products: 6.55 us -> none  [attend(): expo = jnp.exp(scores - peak)]
    all_gather x2 -> x0, blocking collectives: 6.01 us -> none  [body(): lax.all_gather(attended, 'tp', axis=1, tiled=True)]
    reshape x6 -> x0, local copies, waits for them, and re-layouts: 4.58 us -> none  [the longest x2 2.4 us: band_bias(): tiled[:, SEG - 1:SEG - 1 + SEG * (period - 1)]]
    unnamed x28 -> x13, local copies, waits for them, and re-layouts: 2.99 us -> 7.34 us
  transfers between devices with their start and end apart: 4 -> 0, of which waited for: 2 -> 0; matrix products, arithmetic and copies ran while one was open for 21% -> 0% of each run, Pallas kernels for 0% -> 0%
where the time goes in v1:
time: 30.2 us; the launch traced here: 29.8 us
  Pallas kernels  22.4 us (74%)
  local copies, waits for them, and re-layouts  7.34 us (24%)
    pallas_call x1, Pallas kernels, body(): pl.pallas_call(functools.partial(kernel, sp_count, heads), out_shape=jax....  22.4 us
    unnamed x13, local copies, waits for them, and re-layouts  7.34 us

profile of v1, /device:TPU:25, one launch (start us, length us, event | category | flops | bytes accessed | tf_op | source)
XLA Modules:
  0.0 29.8 jit_solution(13726607215309333608)
XLA Ops:
  0.0 0.0 copy-start
  0.0 1.6 %copy-done = bf16[2,2048,256]{2,1,0:T(8,128)(2,1)S(1)} copy-done((bf16[2,2048,256]{2,1,0:T(8,128)(2,1)S(1)}, bf16[2,2048,256]{2,1,0:T(8,128)(2,1)}, u32[]{:S(2)}) %copy-start) | copy-done | bytes 2097176
  1.6 0.0 copy-start.1
  1.6 1.6 %copy-done.1 = bf16[2,2048,256]{2,1,0:T(8,128)(2,1)S(1)} copy-done((bf16[2,2048,256]{2,1,0:T(8,128)(2,1)S(1)}, bf16[2,2048,256]{2,1,0:T(8,128)(2,1)}, u32[]{:S(2)}) %copy-start.1) | copy-done | bytes 2097176
  3.2 0.0 copy-start.2
  3.2 1.2 %copy-done.2 = bf16[256,2048]{1,0:T(8,128)(2,1)S(1)} copy-done((bf16[256,2048]{1,0:T(8,128)(2,1)S(1)}, bf16[256,2048]{1,0:T(8,128)(2,1)}, u32[]{:S(2)}) %copy-start.2) | copy-done | bytes 1048600
  4.4 0.0 copy-start.3
  4.4 0.7 %copy-done.3 = f32[2,2048]{1,0:T(2,128)S(1)} copy-done((f32[2,2048]{1,0:T(2,128)S(1)}, f32[2,2048]{1,0:T(2,128)}, u32[]{:S(2)}) %copy-start.3) | copy-done | bytes 16408
  5.1 0.0 copy-start.4
  5.1 0.7 %copy-done.4 = f32[2,2048]{1,0:T(2,128)S(1)} copy-done((f32[2,2048]{1,0:T(2,128)S(1)}, f32[2,2048]{1,0:T(2,128)}, u32[]{:S(2)}) %copy-start.4) | copy-done | bytes 16408
  5.8 0.0 copy-start.5
  5.8 0.7 %copy-done.5 = f32[2,4,257]{2,1,0:T(4,128)S(1)} copy-done((f32[2,4,257]{2,1,0:T(4,128)S(1)}, f32[2,4,257]{2,1,0:T(4,128)}, u32[]{:S(2)}) %copy-start.5) | copy-done | bytes 8248
  6.6 22.4 %shard_map.82 = bf16[256,1024]{1,0:T(8,128)(2,1)S(1)} custom-call(bf16[256,2048]{1,0:T(8,128)(2,1)S(1)} %copy-done.2, bf16[2,2048,256]{2,1,0:T(8,128)(2,1)S(1)} %copy-done, bf16[2,2048,256]{2,1,0:T(8,128)(2,1)S(1)} %copy-done.1, bf16[2,2048,256]{2,1,0:T(8,128)(2,1)} %wv_hbm.1, bf16[2,512,2048]{2,1,0:T(8,128)(2,1)} %wo_hbm.1, f32[2,4,257]{2,1,0:T(4,128)S(1)} %copy-done.5, ...), custom_call_target="tpu_custom_call" | custom-call | tf_op jit(solution)/shard_map/pallas_call | solution.py:280
  29.0 0.8 %copy.10 = bf16[256,1024]{1,0:T(8,128)(2,1)} copy(bf16[256,1024]{1,0:T(8,128)(2,1)S(1)} %shard_map.82) | data formatting | bytes 1048576
Async XLA Ops:
  0.0 1.6 %copy-start = (bf16[2,2048,256]{2,1,0:T(8,128)(2,1)S(1)}, bf16[2,2048,256]{2,1,0:T(8,128)(2,1)}, u32[]{:S(2)}) copy-start(bf16[2,2048,256]{2,1,0:T(8,128)(2,1)} %wq_hbm.1) | copy-start | bytes 6291460
  1.6 1.6 %copy-start.1 = (bf16[2,2048,256]{2,1,0:T(8,128)(2,1)S(1)}, bf16[2,2048,256]{2,1,0:T(8,128)(2,1)}, u32[]{:S(2)}) copy-start(bf16[2,2048,256]{2,1,0:T(8,128)(2,1)} %wk_hbm.1) | copy-start | bytes 6291460
  3.2 1.2 %copy-start.2 = (bf16[256,2048]{1,0:T(8,128)(2,1)S(1)}, bf16[256,2048]{1,0:T(8,128)(2,1)}, u32[]{:S(2)}) copy-start(bf16[256,2048]{1,0:T(8,128)(2,1)} %tokens.1) | copy-start | bytes 3145732
  4.4 0.7 %copy-start.3 = (f32[2,2048]{1,0:T(2,128)S(1)}, f32[2,2048]{1,0:T(2,128)}, u32[]{:S(2)}) copy-start(f32[2,2048]{1,0:T(2,128)} %gain.1) | copy-start | bytes 49156
  5.1 0.7 %copy-start.4 = (f32[2,2048]{1,0:T(2,128)S(1)}, f32[2,2048]{1,0:T(2,128)}, u32[]{:S(2)}) copy-start(f32[2,2048]{1,0:T(2,128)} %shift.1) | copy-start | bytes 49156
  5.8 0.7 %copy-start.5 = (f32[2,4,257]{2,1,0:T(4,128)S(1)}, f32[2,4,257]{2,1,0:T(4,128)}, u32[]{:S(2)}) copy-start(f32[2,4,257]{2,1,0:T(4,128)} %table.1) | copy-start | bytes 24676

commit v2 on v1

v2 whole, which is shorter than its diff:
```python
import functools

import jax
import jax.numpy as jnp
from jax import lax
from jax.experimental import pallas as pl
from jax.experimental.pallas import tpu as pltpu
from jax.sharding import PartitionSpec as P

SEG = 64
LEFT = 4
CLIP = 128
LAYERS = 2
LANES = 128

residual_scale = 2.0**0.5
norm_eps = 1e-05
masked_score = -1e30
MESH = pl.DeviceIdType.MESH


def kernel(
    sp_count,
    heads,
    tokens,
    wq_hbm,
    wk_hbm,
    wv_hbm,
    wo_hbm,
    table_hbm,
    gain_hbm,
    shift_hbm,
    out,
    x0,
    x1,
    wq,
    wk,
    wv,
    wo,
    table,
    gain,
    shift,
    query,
    kx,
    vx,
    att,
    total,
    bias,
    padded,
    x_sem,
    w_sem,
    small_sem,
    halo_send,
    halo_recv,
    pair_send,
    pair_recv,
):
    rows, model = x0.shape
    width = query.shape[2]
    head_size = width // heads
    reach = LEFT * SEG
    band = reach + SEG
    segments = rows // SEG
    sp = lax.axis_index("sp")
    tp = lax.axis_index("tp")
    has_next = sp < sp_count - 1
    has_prev = sp > 0
    late = (segments // 2, segments)
    early = (0, segments // 2)

    def w_copy(kind, layer):
        source = (wk_hbm, wv_hbm, wq_hbm, wo_hbm)[kind]
        target = (wk, wv, wq, wo)[kind]
        return pltpu.make_async_copy(
            source.at[layer], target.at[layer], w_sem.at[kind, layer]
        )

    x_copy = pltpu.make_async_copy(tokens, x0, x_sem)
    small = [
        pltpu.make_async_copy(source, target, small_sem.at[index])
        for index, (source, target) in enumerate(
            ((table_hbm, table), (gain_hbm, gain), (shift_hbm, shift))
        )
    ]

    def halo_copy(kind, layer, seg):
        buffer = (kx, vx)[kind]
        return pltpu.make_async_remote_copy(
            src_ref=buffer.at[layer, pl.ds(reach + seg * SEG, SEG)],
            dst_ref=buffer.at[layer, pl.ds(seg * SEG, SEG)],
            send_sem=halo_send.at[kind, layer, seg],
            recv_sem=halo_recv.at[kind, layer, seg],
            device_id=(jnp.minimum(sp + 1, sp_count - 1), tp),
            device_id_type=MESH,
        )

    def pair_copy(layer, piece):
        first, last = piece
        block = att.at[layer, tp, pl.ds(first * SEG, (last - first) * SEG)]
        return pltpu.make_async_remote_copy(
            src_ref=block,
            dst_ref=block,
            send_sem=pair_send.at[layer, first],
            recv_sem=pair_recv.at[layer, first],
            device_id=(sp, 1 - tp),
            device_id_type=MESH,
        )

    x_copy.start()
    w_copy(0, 0).start()
    w_copy(1, 0).start()

    barrier = pltpu.get_barrier_semaphore()
    pl.semaphore_signal(barrier, inc=1, device_id=(sp, 1 - tp), device_id_type=MESH)

    @pl.when(has_next)
    def _():
        pl.semaphore_signal(barrier, inc=1, device_id=(sp + 1, tp), device_id_type=MESH)

    @pl.when(has_prev)
    def _():
        pl.semaphore_signal(barrier, inc=1, device_id=(sp - 1, tp), device_id_type=MESH)

    @pl.when(jnp.logical_not(has_prev))
    def _():
        for layer in range(LAYERS):
            kx[layer, :reach, :] = jnp.zeros((reach, width), jnp.bfloat16)
            vx[layer, :reach, :] = jnp.zeros((reach, width), jnp.bfloat16)

    lane = lax.broadcasted_iota(jnp.int32, (1, width), 1)
    in_head = [
        (lane >= h * head_size) & (lane < (h + 1) * head_size) for h in range(heads)
    ]

    def build_bias():
        wide = bias.shape[2]
        size = padded.shape[1]
        padded[...] = jnp.zeros_like(padded)
        for layer in range(LAYERS):
            padded[layer * heads : (layer + 1) * heads, : table.shape[2]] = table[layer]
        place = lax.broadcasted_iota(jnp.int32, (size, wide), 1)
        source = lax.broadcasted_iota(jnp.int32, (size, wide), 0)
        onehot = (jnp.clip(band - 1 - place, -CLIP, CLIP) + CLIP == source).astype(jnp.float32)
        by_offset = jnp.dot(
            padded[...],
            onehot,
            precision=lax.Precision.HIGHEST,
            preferred_element_type=jnp.float32,
        )
        for layer in range(LAYERS):
            for h in range(heads):
                line = by_offset[layer * heads + h : layer * heads + h + 1, :]
                skewed = pltpu.roll(
                    jnp.broadcast_to(line, (SEG, wide)), wide - SEG + 1, 1, stride=1, stride_axis=0
                )
                bias[layer, h * SEG : (h + 1) * SEG, :] = skewed

    def project(hidden, layer, piece, kind):
        part = slice(piece[0] * SEG, piece[1] * SEG)
        weight = (wk, wv, wq)[kind]
        return jnp.dot(
            hidden[part, :], weight[layer], preferred_element_type=jnp.float32
        ).astype(jnp.bfloat16)

    def keys(hidden, layer, piece):
        part = slice(reach + piece[0] * SEG, reach + piece[1] * SEG)
        kx[layer, part, :] = project(hidden, layer, piece, 0)

        @pl.when(has_next)
        def _():
            halo_copy(0, layer, piece[1] - 1).start()

    def values(hidden, layer, piece):
        part = slice(reach + piece[0] * SEG, reach + piece[1] * SEG)
        vx[layer, part, :] = project(hidden, layer, piece, 1)

        @pl.when(has_next)
        def _():
            halo_copy(1, layer, piece[1] - 1).start()
            for seg in range(piece[0], piece[1] - 1)[::-1]:
                halo_copy(0, layer, seg).start()
                halo_copy(1, layer, seg).start()

    def queries(hidden, layer, piece):
        part = slice(piece[0] * SEG, piece[1] * SEG)
        query[layer, part, :] = project(hidden, layer, piece, 2) * jnp.bfloat16(head_size**-0.5)

    def attend(layer, seg):
        @pl.when(has_prev)
        def _():
            halo_copy(0, layer, seg).wait_recv()
            halo_copy(1, layer, seg).wait_recv()

        column = lax.broadcasted_iota(jnp.int32, (1, band), 1)
        block = query[layer, seg * SEG : (seg + 1) * SEG, :]
        stacked = jnp.concatenate(
            [jnp.where(in_head[h], block, jnp.zeros_like(block)) for h in range(heads)], axis=0
        )
        key_band = kx[layer, seg * SEG : seg * SEG + band, :]
        value_band = vx[layer, seg * SEG : seg * SEG + band, :]
        scores = lax.dot_general(
            stacked, key_band, (((1,), (1,)), ((), ())), preferred_element_type=jnp.float32
        )
        outside = (column < reach - seg * SEG) & jnp.logical_not(has_prev)
        scores = jnp.where(outside, masked_score, scores + bias[layer, :, :band])
        peak = jnp.max(scores, -1, keepdims=True)
        expo = jnp.exp(scores - peak)
        norm = jnp.sum(expo, -1, keepdims=True)
        mixed = jnp.dot(
            expo.astype(jnp.bfloat16), value_band, preferred_element_type=jnp.float32
        )
        mixed = mixed * (1.0 / norm)
        own = mixed[:SEG, :]
        for h in range(1, heads):
            own = jnp.where(in_head[h], mixed[h * SEG : (h + 1) * SEG, :], own)
        att[layer, tp, seg * SEG : (seg + 1) * SEG, :] = own.astype(jnp.bfloat16)

    def finish(hidden, layer, piece):
        part = slice(piece[0] * SEG, piece[1] * SEG)
        count = (piece[1] - piece[0]) * SEG

        def half(owner):
            weight = wo[layer, pl.ds(pl.multiple_of(owner * width, width), width), :]
            return jnp.dot(att[layer, owner, part, :], weight, preferred_element_type=jnp.float32)

        total[:count, :] = half(tp)
        pair_copy(layer, piece).wait_recv()
        total[:count, :] += half(1 - tp)
        step = 16
        for r in range(0, count, step):
            here = slice(piece[0] * SEG + r, piece[0] * SEG + r + step)
            value = total[r : r + step, :] + residual_scale * hidden[here, :].astype(jnp.float32)
            mean = jnp.sum(value, -1, keepdims=True) * (1.0 / model)
            centred = value - mean
            variance = jnp.sum(centred * centred, -1, keepdims=True) * (1.0 / model)
            scale = lax.rsqrt(variance + norm_eps)
            if layer < LAYERS - 1:
                x1[here, :] = (
                    centred * scale * gain[layer : layer + 1, :] + shift[layer : layer + 1, :]
                ).astype(jnp.bfloat16)
            else:
                cols = pl.ds(pl.multiple_of(tp * (model // 2), model // 2), model // 2)
                value = total[r : r + step, cols] + residual_scale * hidden[here, cols].astype(
                    jnp.float32
                )
                out[here, :] = (
                    (value - mean) * scale * gain[layer : layer + 1, cols]
                    + shift[layer : layer + 1, cols]
                ).astype(jnp.bfloat16)

    every = (0, segments)
    x_copy.wait()
    w_copy(0, 0).wait()
    for copy in (w_copy(2, 0), w_copy(3, 0), *small):
        copy.start()
    pl.semaphore_wait(barrier, 1 + has_next.astype(jnp.int32) + has_prev.astype(jnp.int32))
    keys(x0, 0, every)
    w_copy(1, 0).wait()
    values(x0, 0, every)
    w_copy(2, 0).wait()
    queries(x0, 0, every)
    for kind in range(4):
        w_copy(kind, 1).start()
    for copy in small:
        copy.wait()
    build_bias()
    w_copy(3, 0).wait()
    for kind in range(4):
        w_copy(kind, 1).wait()

    for seg in range(*late)[::-1]:
        attend(0, seg)
    pair_copy(0, late).start()
    for seg in range(early[0] + 1, early[1])[::-1]:
        attend(0, seg)
    finish(x0, 0, late)
    keys(x1, 1, late)
    values(x1, 1, late)
    attend(0, 0)
    pair_copy(0, early).start()
    queries(x1, 1, late)
    finish(x0, 0, early)
    keys(x1, 1, early)
    values(x1, 1, early)
    queries(x1, 1, early)

    for seg in range(*late)[::-1]:
        attend(1, seg)
    pair_copy(1, late).start()
    pieces = [(seg, seg + 1) for seg in range(*early)[::-1]]
    waiting = late
    for piece in pieces:
        attend(1, piece[0])
        pair_copy(1, piece).start()
        finish(x1, 1, waiting)
        waiting = piece
    finish(x1, 1, waiting)

    for layer, piece in [(0, late), (0, early), (1, late)] + [(1, piece) for piece in pieces]:
        pair_copy(layer, piece).wait_send()

    @pl.when(has_next)
    def _():
        for layer in range(LAYERS):
            for seg in range(segments):
                for kind in range(2):
                    halo_copy(kind, layer, seg).wait_send()


def body(
    sp_count, tokens, query_weight, key_weight, value_weight, out_weight, rel_table, norm_gain,
    norm_bias,
):
    rows, model = tokens.shape
    width = query_weight.shape[2]
    heads = rel_table.shape[1]
    reach = LEFT * SEG
    segments = rows // SEG
    wide = -(-(reach + 2 * SEG - 1) // LANES) * LANES
    size = -(-rel_table.shape[2] // LANES) * LANES
    hbm = pl.BlockSpec(memory_space=pltpu.MemorySpace.HBM)
    vmem = pl.BlockSpec(memory_space=pltpu.VMEM)
    bf16 = jnp.bfloat16
    return pl.pallas_call(
        functools.partial(kernel, sp_count, heads),
        out_shape=jax.ShapeDtypeStruct((rows, model // 2), bf16),
        in_specs=[hbm] * 8,
        out_specs=vmem,
        scratch_shapes=[
            pltpu.VMEM((rows, model), bf16),
            pltpu.VMEM((rows, model), bf16),
            pltpu.VMEM(query_weight.shape, bf16),
            pltpu.VMEM(key_weight.shape, bf16),
            pltpu.VMEM(value_weight.shape, bf16),
            pltpu.VMEM(out_weight.shape, bf16),
            pltpu.VMEM(rel_table.shape, jnp.float32),
            pltpu.VMEM(norm_gain.shape, jnp.float32),
            pltpu.VMEM(norm_bias.shape, jnp.float32),
            pltpu.VMEM((LAYERS, rows, width), bf16),
            pltpu.VMEM((LAYERS, reach + rows, width), bf16),
            pltpu.VMEM((LAYERS, reach + rows, width), bf16),
            pltpu.VMEM((LAYERS, 2, rows, width), bf16),
            pltpu.VMEM((rows // 2, model), jnp.float32),
            pltpu.VMEM((LAYERS, heads * SEG, wide), jnp.float32),
            pltpu.VMEM((-(-LAYERS * heads // 8) * 8, size), jnp.float32),
            pltpu.SemaphoreType.DMA,
            pltpu.SemaphoreType.DMA((4, LAYERS)),
            pltpu.SemaphoreType.DMA((3,)),
            pltpu.SemaphoreType.DMA((2, LAYERS, segments)),
            pltpu.SemaphoreType.DMA((2, LAYERS, segments)),
            pltpu.SemaphoreType.DMA((LAYERS, segments)),
            pltpu.SemaphoreType.DMA((LAYERS, segments)),
        ],
        compiler_params=pltpu.CompilerParams(
            collective_id=0, has_side_effects=True, vmem_limit_bytes=65950000
        ),
    )(
        tokens, query_weight, key_weight, value_weight, out_weight, rel_table, norm_gain, norm_bias
    )


def solution(mesh):
    return jax.shard_map(
        functools.partial(body, mesh.shape["sp"]),
        mesh=mesh,
        in_specs=(
            P("sp", None),
            P(None, None, "tp"),
            P(None, None, "tp"),
            P(None, None, "tp"),
            P(),
            P(None, "tp", None),
            P(),
            P(),
        ),
        out_specs=P("sp", "tp"),
        check_vma=False,
    )
```

time: 30.2 us -> 25.5 us (0.84); the launches traced: 29.8 us -> 25.4 us
  local copies, waits for them, and re-layouts: 7.34 us -> 1.87 us
  Pallas kernels: 22.4 us -> 23.5 us
    unnamed x13 -> x1, local copies, waits for them, and re-layouts: 7.34 us -> 1.87 us
    pallas_call x1, Pallas kernels: 22.4 us -> 23.5 us  [body(): pl.pallas_call(functools.partial(kernel, sp_count, heads), out_shape=jax....]
where the time goes in v2:
time: 25.5 us; the launch traced here: 25.4 us
  Pallas kernels  23.5 us (92%)
  local copies, waits for them, and re-layouts  1.87 us (7%)
    pallas_call x1, Pallas kernels, body(): pl.pallas_call(functools.partial(kernel, sp_count, heads), out_shape=jax....  23.5 us
    unnamed x1, local copies, waits for them, and re-layouts  1.87 us

profile of v2, /device:TPU:25, one launch (start us, length us, event | category | flops | bytes accessed | tf_op | source)
XLA Modules:
  0.0 25.4 jit_solution(14776089539556938537)
XLA Ops:
  0.0 23.5 %shard_map.82 = bf16[256,1024]{1,0:T(8,128)(2,1)} custom-call(bf16[256,2048]{1,0:T(8,128)(2,1)} %tokens.1, bf16[2,2048,256]{2,1,0:T(8,128)(2,1)} %wq_hbm.1, bf16[2,2048,256]{2,1,0:T(8,128)(2,1)} %wk_hbm.1, bf16[2,2048,256]{2,1,0:T(8,128)(2,1)} %wv_hbm.1, bf16[2,512,2048]{2,1,0:T(8,128)(2,1)} %wo_hbm.1, f32[2,4,257]{2,1,0:T(4,128)} %table_hbm.1, ...), custom_call_target="tpu_custom_call" | custom-call | tf_op jit(solution)/shard_map/pallas_call | solution.py:324
  23.5 1.9 %copy.10 = bf16[256,1024]{1,0:T(8,128)(2,1)} copy(bf16[256,1024]{1,0:T(8,128)(2,1)} %shard_map.82) | data formatting | bytes 1048576

commit v3 on v2

--- a/solution.py
+++ b/solution.py
@@ -223,13 +223,13 @@
             weight = wo[layer, pl.ds(pl.multiple_of(owner * width, width), width), :]
             return jnp.dot(att[layer, owner, part, :], weight, preferred_element_type=jnp.float32)
 
-        total[:count, :] = half(tp)
+        total[:count, :] = half(tp) + residual_scale * hidden[part, :].astype(jnp.float32)
         pair_copy(layer, piece).wait_recv()
         total[:count, :] += half(1 - tp)
         step = 16
         for r in range(0, count, step):
             here = slice(piece[0] * SEG + r, piece[0] * SEG + r + step)
-            value = total[r : r + step, :] + residual_scale * hidden[here, :].astype(jnp.float32)
+            value = total[r : r + step, :]
             mean = jnp.sum(value, -1, keepdims=True) * (1.0 / model)
             centred = value - mean
             variance = jnp.sum(centred * centred, -1, keepdims=True) * (1.0 / model)
@@ -240,11 +240,8 @@
                 ).astype(jnp.bfloat16)
             else:
                 cols = pl.ds(pl.multiple_of(tp * (model // 2), model // 2), model // 2)
-                value = total[r : r + step, cols] + residual_scale * hidden[here, cols].astype(
-                    jnp.float32
-                )
                 out[here, :] = (
-                    (value - mean) * scale * gain[layer : layer + 1, cols]
+                    (total[r : r + step, cols] - mean) * scale * gain[layer : layer + 1, cols]
                     + shift[layer : layer + 1, cols]
                 ).astype(jnp.bfloat16)
 
@@ -265,8 +262,6 @@
         copy.wait()
     build_bias()
     w_copy(3, 0).wait()
-    for kind in range(4):
-        w_copy(kind, 1).wait()
 
     for seg in range(*late)[::-1]:
         attend(0, seg)
@@ -274,10 +269,14 @@
     for seg in range(early[0] + 1, early[1])[::-1]:
         attend(0, seg)
     finish(x0, 0, late)
+    w_copy(0, 1).wait()
+    w_copy(1, 1).wait()
     keys(x1, 1, late)
     values(x1, 1, late)
     attend(0, 0)
     pair_copy(0, early).start()
+    w_copy(2, 1).wait()
+    w_copy(3, 1).wait()
     queries(x1, 1, late)
     finish(x0, 0, early)
     keys(x1, 1, early)
@@ -352,10 +351,22 @@
             pltpu.SemaphoreType.DMA((LAYERS, segments)),
         ],
         compiler_params=pltpu.CompilerParams(
-            collective_id=0, has_side_effects=True, vmem_limit_bytes=65950000
+            collective_id=0, has_side_effects=True, vmem_limit_bytes=56000000
         ),
     )(
-        tokens, query_weight, key_weight, value_weight, out_weight, rel_table, norm_gain, norm_bias
+        *(
+            pltpu.with_memory_space_constraint(operand, pltpu.MemorySpace.HBM)
+            for operand in (
+                tokens,
+                query_weight,
+                key_weight,
+                value_weight,
+                out_weight,
+                rel_table,
+                norm_gain,
+                norm_bias,
+            )
+        )
     )
 
 

time: 25.5 us -> 23.6 us (0.925)
  local copies, waits for them, and re-layouts: 1.87 us -> 0.8 us
  Pallas kernels: 23.5 us -> 22.7 us
    unnamed x1, local copies, waits for them, and re-layouts: 1.87 us -> 0.8 us
    pallas_call x1, Pallas kernels: 23.5 us -> 22.7 us  [body(): pl.pallas_call(functools.partial(kernel, sp_count, heads), out_shape=jax....]
where the time goes in v3:
time: 23.6 us; the launch traced here: 23.5 us
  Pallas kernels  22.7 us (96%)
  local copies, waits for them, and re-layouts  0.8 us (3%)
    pallas_call x1, Pallas kernels, body(): pl.pallas_call(functools.partial(kernel, sp_count, heads), out_shape=jax....  22.7 us
    unnamed x1, local copies, waits for them, and re-layouts  0.8 us

profile of v3, /device:TPU:25, one launch (start us, length us, event | category | flops | bytes accessed | tf_op | source)
XLA Modules:
  0.0 23.5 jit_solution(11361761935228691951)
XLA Ops:
  0.0 22.7 %shard_map.82 = bf16[256,1024]{1,0:T(8,128)(2,1)S(1)} custom-call(bf16[256,2048]{1,0:T(8,128)(2,1)} %tokens.1, bf16[2,2048,256]{2,1,0:T(8,128)(2,1)} %wq_hbm.1, bf16[2,2048,256]{2,1,0:T(8,128)(2,1)} %wk_hbm.1, bf16[2,2048,256]{2,1,0:T(8,128)(2,1)} %wv_hbm.1, bf16[2,512,2048]{2,1,0:T(8,128)(2,1)} %wo_hbm.1, f32[2,4,257]{2,1,0:T(4,128)} %table_hbm.1, ...), custom_call_target="tpu_custom_call" | custom-call | tf_op jit(solution)/shard_map/pallas_call | solution.py:323
  22.7 0.8 %copy.10 = bf16[256,1024]{1,0:T(8,128)(2,1)} copy(bf16[256,1024]{1,0:T(8,128)(2,1)S(1)} %shard_map.82) | data formatting | bytes 1048576
